TPU v7x, 256 devices: a 4x2x16 block of a 4x16x16 slice. The times are simulated.
256 devices in a mesh: grp: 2 (over y), fs: 16 (over z), tp: 8 (over x, core).
Axes of the slice: x: 4, y: 2, z: 16, core: 2. Of those that a mesh axis runs over, the one named last changes fastest.
The devices are a block of a 4x16x16 slice.
Arguments:
- tokens: bfloat16 [32768, 2048], P(('grp', 'fs', 'tp')), parts along dimension 0, may hold values from -6 to 6
- norm_gains: float32 [4, 2048], replicated, may hold values from 0.1 to 1.9
- query_weight: bfloat16 [2048, 2048], P('fs', 'tp'), may hold values from -0.125 to 0.125
- key_weight: bfloat16 [2048, 2048], P('fs', 'tp'), may hold values from -0.125 to 0.125
- value_weight: bfloat16 [2048, 4096], P('fs', 'tp'), may hold values from -0.125 to 0.125
- swish_weight: bfloat16 [2048, 4096], P('fs', 'tp'), may hold values from -0.125 to 0.125
- mixer_output: bfloat16 [4096, 2048], P('tp', 'fs'), may hold values from -0.09375 to 0.09375
- gate_weight: bfloat16 [2048, 3072], P('fs', 'tp'), may hold values from -0.125 to 0.125
- up_weight: bfloat16 [2048, 3072], P('fs', 'tp'), may hold values from -0.125 to 0.125
- down_weight: bfloat16 [3072, 2048], P('tp', 'fs'), may hold values from -0.109375 to 0.109375
Outputs:
- layer_output: bfloat16 [32768, 2048], P(('grp', 'fs', 'tp')), parts along dimension 0
There are 2 independent parts, one for each index of `grp`. A program takes and returns all parts, laid end to end along the dimension named above; an argument that names none is the same for every part. Nothing has to cross between parts.
All inputs are finite; a program needn't handle non-finite values.
Results may differ from a plain program's by a relative error of at most 0.02.
Values may be sent and summed in bfloat16 or wider, within the bound.
A program may use at most 64 MiB of HBM per device.

v0:
```python
import jax
import jax.numpy as jnp
from jax import lax
from jax.sharding import PartitionSpec as P

H = 8
QK = 256
BLOCK = 128
norm_epsilon = 1e-06
group_epsilon = 0.01


def laid_out(pieces, dim):
    lengths = list(pieces.shape[1:])
    lengths[dim] *= pieces.shape[0]
    return jnp.moveaxis(pieces, 0, dim).reshape(lengths)


def from_everyone(array, axis):
    copies = jnp.broadcast_to(array, (lax.axis_size(axis), *array.shape))
    return lax.all_to_all(copies, axis, split_axis=0, concat_axis=0, tiled=True)


def gather_directly(array, axis, dim):
    return laid_out(from_everyone(array, axis), dim)


def split_up(array, dim, count):
    before, after = (array.shape[:dim], array.shape[dim + 1 :])
    return jnp.moveaxis(array.reshape(*before, count, -1, *after), dim, 0)


def summed_on_arrival(array, axis, dim):
    count = lax.axis_size(axis)
    pieces = lax.all_to_all(split_up(array, dim, count), axis, 0, 0, tiled=True)
    return jnp.sum(pieces.astype(jnp.float32), axis=0)


def sent_together(arrays, axis, dim, along):
    ends, at = ([], 0)
    for a in arrays[:-1]:
        at += a.shape[along]
        ends.append(at)
    both = jnp.concatenate(arrays, axis=along)
    return tuple(jnp.split(lax.all_gather(both, axis, axis=dim, tiled=True), ends, axis=along))


def rms_scale(matrix, gain):
    return (
        matrix * lax.rsqrt(jnp.mean(matrix * matrix, axis=-1, keepdims=True) + norm_epsilon) * gain
    )


def gather_rows(normed):
    return lax.all_gather(normed, "tp", axis=0, tiled=True)


def add_piece(normed, shard_piece):
    return jnp.dot(normed, shard_piece, preferred_element_type=jnp.float32)


def project_out(active, weight_shard):
    whole_weight = gather_directly(weight_shard, "fs", 1)
    return summed_on_arrival(
        jnp.dot(active, whole_weight, preferred_element_type=jnp.float32).astype(jnp.bfloat16),
        "tp",
        0,
    )


def rotate_halves(head_tensors, cosine_table, sine_table):
    half_width = head_tensors.shape[-1] // 2
    lower_half = head_tensors[..., :half_width]
    upper_half = head_tensors[..., half_width:]
    return jnp.concatenate(
        [
            lower_half * cosine_table - upper_half * sine_table,
            lower_half * sine_table + upper_half * cosine_table,
        ],
        axis=-1,
    )


def retention(queries, key_rows, value_rows, log_decay):
    length, head_count, key_width = queries.shape
    value_width = value_rows.shape[-1]
    blocks = length // BLOCK
    query_blocks = queries.reshape(blocks, BLOCK, head_count, key_width)
    key_blocks = key_rows.reshape(blocks, BLOCK, head_count, key_width)
    value_blocks = value_rows.reshape(blocks, BLOCK, head_count, value_width)
    offsets = jnp.arange(BLOCK, dtype=jnp.float32)
    distance = offsets[:, None] - offsets[None, :]
    within = jnp.where(
        distance >= 0, jnp.exp(log_decay[:, None, None] * jnp.maximum(distance, 0.0)), 0.0
    )
    retention_scores = jnp.einsum(
        "cnhd,cmhd->chnm", query_blocks, key_blocks, preferred_element_type=jnp.float32
    )
    local_part = jnp.einsum(
        "chnm,cmhe->cnhe", retention_scores * within[None], value_blocks.astype(jnp.float32)
    )
    key_decay = jnp.exp((BLOCK - 1.0 - offsets)[:, None] * log_decay[None, :])
    query_decay = jnp.exp((offsets + 1.0)[:, None] * log_decay[None, :])
    block_decay = jnp.exp(BLOCK * log_decay)

    def advance(carry_state, inputs):
        query_block, key_block, value_tile = inputs
        carried = (
            jnp.einsum("nhd,hde->nhe", query_block.astype(jnp.float32), carry_state)
            * query_decay[:, :, None]
        )
        decay_weighted = key_block.astype(jnp.float32) * key_decay[:, :, None]
        carry_state = carry_state * block_decay[:, None, None] + jnp.einsum(
            "yui,yua->uia", decay_weighted, value_tile.astype(jnp.float32)
        )
        return (carry_state, carried)

    starting_state = jnp.zeros((head_count, key_width, value_width), jnp.float32)
    _, carried = lax.scan(advance, starting_state, (query_blocks, key_blocks, value_blocks))
    return (local_part + carried).reshape(length, head_count, value_width)


def per_device(
    tokens,
    norm_gains,
    query_weight,
    key_weight,
    value_weight,
    swish_weight,
    mixer_output,
    gate_weight,
    up_weight,
    down_weight,
):
    residual = tokens.astype(jnp.float32)
    normed = gather_rows(rms_scale(residual, norm_gains[0]).astype(jnp.bfloat16))
    gate_whole, up_whole = sent_together((gate_weight, up_weight), "fs", 0, 1)
    pieces = sent_together((query_weight, key_weight, value_weight, swish_weight), "fs", 0, 1)
    raw_query, raw_keys, raw_values, raw_swish = tuple(
        (add_piece(normed, shard_piece) for shard_piece in pieces)
    )
    length = normed.shape[0]
    head_count = raw_query.shape[1] // QK
    positions = jnp.arange(length, dtype=jnp.float32)
    frequency = 10000.0 ** (-jnp.linspace(0.0, 1.0, QK // 2, dtype=jnp.float32))
    angles = positions[:, None] * frequency[None, :]
    cosine_table = jnp.cos(angles)[:, None, :]
    sine_table = jnp.sin(angles)[:, None, :]
    queries = rotate_halves(
        raw_query.reshape(length, head_count, QK), cosine_table, sine_table
    ).astype(jnp.bfloat16)
    key_rows = (
        rotate_halves(raw_keys.reshape(length, head_count, QK), cosine_table, sine_table)
        * QK ** (-0.5)
    ).astype(jnp.bfloat16)
    value_rows = raw_values.reshape(length, head_count, -1).astype(jnp.bfloat16)
    head_index = (lax.axis_index("tp") * head_count + jnp.arange(head_count)).astype(jnp.float32)
    log_decay = -(4.0 / BLOCK) * (BLOCK / (32.0 * length)) ** (head_index / (H - 1))
    retained = retention(queries, key_rows, value_rows, log_decay)
    centred = retained - jnp.mean(retained, axis=-1, keepdims=True)
    normalized = centred * lax.rsqrt(
        jnp.mean(centred * centred, axis=-1, keepdims=True) + group_epsilon
    )
    gated_rows = (jax.nn.silu(raw_swish) * normalized.reshape(length, -1)).astype(jnp.bfloat16)
    mixer_total = project_out(gated_rows, mixer_output)
    after_mixer = residual + rms_scale(mixer_total, norm_gains[1])
    widened = gather_rows(rms_scale(after_mixer, norm_gains[2]).astype(jnp.bfloat16))
    gate_sum = jnp.dot(widened, gate_whole, preferred_element_type=jnp.float32)
    up_sum = jnp.dot(widened, up_whole, preferred_element_type=jnp.float32)
    hidden = (jax.nn.silu(gate_sum) * up_sum).astype(jnp.bfloat16)
    channel = project_out(hidden, down_weight)
    return (after_mixer + rms_scale(channel, norm_gains[3])).astype(jnp.bfloat16)


def solution(mesh):
    placed = (
        P(("grp", "fs", "tp"), None),
        P(),
        P("fs", "tp"),
        P("fs", "tp"),
        P("fs", "tp"),
        P("fs", "tp"),
        P("tp", "fs"),
        P("fs", "tp"),
        P("fs", "tp"),
        P("tp", "fs"),
    )
    return jax.shard_map(
        per_device,
        mesh=mesh,
        in_specs=placed,
        out_specs=P(("grp", "fs", "tp"), None),
        check_vma=False,
    )
```

profile of v0, /device:TPU:33, one launch (start us, length us, event | category | flops | bytes accessed | tf_op | source)
XLA Modules:
  0.0 461.9 jit_solution(14256166903097563935)
XLA Ops:
  6.6 1.0 fusion.72
  7.6 1.2 fusion.39
  8.8 2.0 fusion.41
  11.0 0.8 pad_maximum_fusion.1
  12.0 1.5 broadcast_in_dim.19
  13.5 24.7 %all-to-all-start = ((bf16[16,512,128]{1,2,0:T(8,128)(2,1)}), bf16[16,512,128]{1,2,0:T(8,128)(2,1)}, u32[]{:S(2)}, u32[]{:S(2)}) async-start(bf16[16,512,128]{1,2,0:T(8,128)(2,1)} %broadcast_in_dim.19), calls=%async_computation | async-start | bytes 4194304 | tf_op jit(solution)/shard_map/all_to_all | solution.py:21
  38.3 0.7 pad_maximum_fusion.2
  39.4 24.8 %all-gather.5.cloned.1.call-done = bf16[1024,2048]{1,0:T(8,128)(2,1)} async-done(((bf16[128,2048]{1,0:T(8,128)(2,1)}), bf16[1024,2048]{1,0:T(8,128)(2,1)}) %all-gather.5.cloned.1.call-update) | async-done | bytes 4194320 | tf_op jit(solution)/shard_map/all_gather | solution.py:55
  64.2 130.5 %all-gather.7.cloned.1.call-done = bf16[2048,1536]{1,0:T(8,128)(2,1)} async-done(((bf16[128,1536]{1,0:T(8,128)(2,1)}), bf16[2048,1536]{1,0:T(8,128)(2,1)}) %all-gather.7.cloned.1.call-update) | async-done | bytes 6291472 | tf_op jit(solution)/shard_map/all_gather | solution.py:45
  194.7 3.9 convolution_bitcast_fusion.2
  198.6 0.5 copy-done.10
  199.1 3.4 convolution_bitcast_fusion.3
  202.5 2.3 subtract_convert_fusion
  204.8 0.9 pad_maximum_fusion
  205.7 1.1 fusion.45
  206.8 3.3 fusion.36
  210.1 25.3 %while.15 = (s32[]{:T(128)}, f32[1,256,512]{2,1,0:T(8,128)S(1)}, f32[8,128,1,512]{3,1,2,0:T(8,128)}, f32[1]{0:T(128)}, bf16[8,128,1,256]{3,2,1,0:T(2,128)(2,1)S(...) while((s32[]{:T(128)}, f32[1,256,512]{2,1,0:T(8,128)S(1)}, ...), condition=%wide.region_2.3_spmd.clone.clone.clone, body=%wide.region_1.2_spmd.clone.clone.clone.sunk | while | flops 67797504 | bytes 2232440 | solution.py:119
  210.2 1.7 fusion.99
  212.1 1.2 fusion.98
  213.3 1.8 fusion.99
  215.3 1.2 fusion.98
  216.5 1.7 fusion.99
  218.5 1.2 fusion.98
  219.7 1.7 fusion.99
  221.6 1.2 fusion.98
  222.8 1.7 fusion.99
  224.8 1.2 fusion.98
  226.0 1.7 fusion.99
  228.0 1.2 fusion.98
  229.2 1.8 fusion.99
  231.1 1.2 fusion.98
  232.3 1.7 fusion.99
  234.3 1.2 fusion.98
  235.5 2.7 fusion.73
  238.6 5.6 %fusion.27 = bf16[1024,512]{1,0:T(8,128)(2,1)S(1)} fusion(f32[8,128,1,512]{3,1,0,2:T(8,128)S(1)} %get-tuple-element.179, bf16[1024,2048]{1,0:T(8,128)(2,1)} %all-gather.5.cloned.1.call-done, bf16[2048,1536]{1,0:T(8,128)(2,1)} %all-gather.7.cloned.1.call-done, f32[1024]{0:T(1024)S(1)} %rsqrt_bitcast_fusion, f32[1024]{0:T(1024)S(1)} %get-tuple-element.174), kind=kOutput, calls=%fused_computation.36 | convolution fusion | flops 2151677952 | bytes 9445376 | tf_op jit(solution)/shard_map/dot_general | solution.py:59
  244.2 4.0 convolution_convert_fusion.1
  248.2 56.0 %all_to_all.20 = bf16[8,128,2048]{2,1,0:T(8,128)(2,1)S(1)} all-to-all(bf16[8,128,2048]{2,1,0:T(8,128)(2,1)S(1)} %bitcast.130), channel_id=1, replica_groups=mesh['grp'=2,'fs'=16,'tp'=8] {'tp'}, dimensions={0} | all-to-all | bytes 8388608 | tf_op jit(solution)/shard_map/all_to_all | solution.py:35
  304.2 0.7 convert_reduce_fusion.1
  305.6 1.1 multiply_convert_fusion.1
  306.9 1.4 broadcast_in_dim.20
  308.3 8.1 %all-to-all-start.2 = ((bf16[16,384,128]{1,2,0:T(8,128)(2,1)}), bf16[16,384,128]{1,2,0:T(8,128)(2,1)S(1)}, u32[]{:S(2)}, u32[]{:S(2)}) async-start(bf16[16,384,128]{1,2,0:T(8,128)(2,1)} %broadcast_in_dim.20), calls=%async_computation.2 | async-start | bytes 3145728 | tf_op jit(solution)/shard_map/all_to_all | solution.py:21
  316.4 25.5 %all-gather.9.cloned.1.call-done = bf16[1024,2048]{1,0:T(8,128)(2,1)} async-done(((bf16[128,2048]{1,0:T(8,128)(2,1)}), bf16[1024,2048]{1,0:T(8,128)(2,1)}) %all-gather.9.cloned.1.call-update) | async-done | bytes 4194320 | tf_op jit(solution)/shard_map/all_gather | solution.py:55
  342.0 6.2 %fusion.30 = f32[1024,384]{1,0:T(8,128)} fusion(bf16[1024,2048]{1,0:T(8,128)(2,1)} %all-gather.9.cloned.1.call-done, bf16[2048,768]{1,0:T(8,128)(2,1)} %all-gather.11.cloned.1.call-done), kind=kOutput, calls=%fused_computation.40 | convolution fusion | flops 1610612736 | bytes 7340032 | tf_op jit(solution)/shard_map/dot_general | solution.py:168
  348.1 37.1 %all-to-all-done.2 = bf16[16,384,128]{1,2,0:T(8,128)(2,1)S(1)} async-done(((bf16[16,384,128]{1,2,0:T(8,128)(2,1)}), bf16[16,384,128]{1,2,0:T(8,128)(2,1)S(1)}, u32[]{:S(2)}, u32[]{:S(2)}) %all-to-all-start.2) | async-done | bytes 1572896 | tf_op jit(solution)/shard_map/all_to_all | solution.py:21
  385.3 9.6 %convolution_convert_fusion = bf16[1024,2048]{1,0:T(8,128)(2,1)} fusion(bf16[384,2048]{0,1:T(8,128)(2,1)S(1)} %bitcast.137, f32[1024,384]{1,0:T(8,128)} %fusion.30, bf16[1024,2048]{1,0:T(8,128)(2,1)} %all-gather.9.cloned.1.call-done, bf16[2048,768]{1,0:T(8,128)(2,1)} %all-gather.11.cloned.1.call-done), kind=kOutput, calls=%fused_computation.26 | convolution fusion | flops 3225681920 | bytes 13107200 | tf_op jit(solution)/shard_map/dot_general | solution.py:65
  394.9 58.4 %all_to_all.21 = bf16[8,128,2048]{2,1,0:T(8,128)(2,1)S(1)} all-to-all(bf16[8,128,2048]{2,1,0:T(8,128)(2,1)} %bitcast.129), channel_id=1, replica_groups=mesh['grp'=2,'fs'=16,'tp'=8] {'tp'}, dimensions={0} | all-to-all | bytes 8388608 | tf_op jit(solution)/shard_map/all_to_all | solution.py:35
  453.2 0.7 convert_reduce_fusion
  454.1 1.2 add_convert_fusion
  (66 shorter events, 3.9 us)
Async XLA Ops:
  6.5 4.4 copy-start.9
  6.5 4.5 copy-start.8
  6.6 4.5 copy-start.4
  6.6 4.5 copy-start.3
  6.6 5.3 %copy-start.2 = (bf16[512,128]{1,0:T(8,128)(2,1)S(1)}, bf16[512,128]{1,0:T(8,128)(2,1)}, u32[]{:S(2)}) copy-start(bf16[512,128]{1,0:T(8,128)(2,1)} %param.18) | copy-start | bytes 393220
  6.6 57.6 %all-gather.5.cloned.1.call-start = ((), (), s32[]{:S(2)}) async-start(), calls=%async_computation.4 | async-start | bytes 4718592 | tf_op jit(solution)/shard_map/all_gather | solution.py:55
  10.9 183.8 %all-gather.7.cloned.1.call-start = ((), (), s32[]{:S(2)}) async-start(), calls=%async_computation.5 | async-start | bytes 6684672 | tf_op jit(solution)/shard_map/all_gather | solution.py:45
  13.5 24.7 %copy-start.6 = (bf16[128,384]{1,0:T(8,128)(2,1)S(1)}, bf16[128,384]{1,0:T(8,128)(2,1)}, u32[]{:S(2)}) copy-start(bf16[128,384]{1,0:T(8,128)(2,1)} %param.20) | copy-start | bytes 294916
  13.5 24.7 %copy-start.7 = (bf16[128,384]{1,0:T(8,128)(2,1)S(1)}, bf16[128,384]{1,0:T(8,128)(2,1)}, u32[]{:S(2)}) copy-start(bf16[128,384]{1,0:T(8,128)(2,1)} %param.19) | copy-start | bytes 294916
  13.5 230.7 %all-to-all-start = ((bf16[16,512,128]{1,2,0:T(8,128)(2,1)}), bf16[16,512,128]{1,2,0:T(8,128)(2,1)}, u32[]{:S(2)}, u32[]{:S(2)}) async-start(bf16[16,512,128]{1,2,0:T(8,128)(2,1)} %broadcast_in_dim.19), calls=%async_computation | async-start | bytes 4194304 | tf_op jit(solution)/shard_map/all_to_all | solution.py:21
  38.2 278.3 %all-gather.11.cloned.1.call-start = ((), (), s32[]{:S(2)}) async-start(), calls=%async_computation.7 | async-start | bytes 3342336 | tf_op jit(solution)/shard_map/all_gather | solution.py:45
  39.0 302.9 %all-gather.9.cloned.1.call-start = ((), (), s32[]{:S(2)}) async-start(), calls=%async_computation.6 | async-start | bytes 4718592 | tf_op jit(solution)/shard_map/all_gather | solution.py:55
  194.7 4.4 copy-start.10
  202.5 4.3 copy-start.11
  204.8 5.3 %copy-start.1 = (bf16[1024,1,128]{2,0,1:T(8,128)(2,1)}, bf16[1024,1,128]{2,0,1:T(8,128)(2,1)S(1)}, u32[]{:S(2)}) copy-start(bf16[1024,1,128]{2,0,1:T(8,128)(2,1)S(1)} %get-tuple-element.167) | copy-start | bytes 786436
  304.2 1.0 copy-start
  305.3 1.5 copy-start.5
  308.3 77.0 %all-to-all-start.2 = ((bf16[16,384,128]{1,2,0:T(8,128)(2,1)}), bf16[16,384,128]{1,2,0:T(8,128)(2,1)S(1)}, u32[]{:S(2)}, u32[]{:S(2)}) async-start(bf16[16,384,128]{1,2,0:T(8,128)(2,1)} %broadcast_in_dim.20), calls=%async_computation.2 | async-start | bytes 3145728 | tf_op jit(solution)/shard_map/all_to_all | solution.py:21
Sparse Core Ops, SparseCore 0:
  11.0 53.0 all-gather.4
  66.0 128.6 all-gather.6
  196.5 65.3 all-gather.10
  306.9 34.9 all-gather.8
where the time goes:
time: 463 us; the launch traced here: 462 us
  waiting for transfers between devices  218 us (47%)
  blocking collectives  114 us (25%)
  matrix products  62 us (13%)
  starting transfers between devices  33 us (7%)
  other arithmetic  15.7 us (3%)
  between operations  13.5 us (3%)
  local copies, waits for them, and re-layouts  4.77 us (1%)
    all_gather x2, waiting for transfers between devices, sent_together(): lax.all_gather(both, axis, axis=dim, tiled=True)  131 us
    all_to_all x2, blocking collectives, summed_on_arrival(): pieces = lax.all_to_all(split_up(array, dim, count), axis, 0, 0, tiled=True)  114 us
    all_gather x2, waiting for transfers between devices, gather_rows(): return lax.all_gather(normed, 'tp', axis=0, tiled=True)  50.3 us
    all_to_all x2, waiting for transfers between devices, from_everyone(): return lax.all_to_all(copies, axis, split_axis=0, concat_axis=0, tiled=True)  37.1 us
    all_to_all x2, starting transfers between devices, from_everyone(): return lax.all_to_all(copies, axis, split_axis=0, concat_axis=0, tiled=True)  32.7 us
    dot_general x4, matrix products, add_piece(): return jnp.dot(normed, shard_piece, preferred_element_type=jnp.float32)  16.2 us
    dot_general x8, matrix products, advance(): jnp.einsum('nhd,hde->nhe', query_block.astype(jnp.float32), carry_state)  14 us
    dot_general x2, matrix products, project_out(): jnp.dot(active, whole_weight, preferred_element_type=jnp.float32)  13.6 us
  transfers between devices with their start and end apart: 6, of which 4 were waited for; matrix products, arithmetic and copies ran while one was open for 14% of the time, Pallas kernels for 0%

commit v1 on v0

--- a/solution.py
+++ b/solution.py
@@ -8,6 +8,19 @@
 BLOCK = 128
 norm_epsilon = 1e-06
 group_epsilon = 0.01
+
+
+def ring_gather(x, axis, dim):
+    ways = lax.axis_size(axis)
+    up = [(d, (d + 1) % ways) for d in range(ways)]
+    down = [(d, (d - 1) % ways) for d in range(ways)]
+    earlier, later = ([x], [x])
+    for _ in range(ways // 2):
+        earlier.append(lax.ppermute(earlier[-1], axis, up))
+    for _ in range((ways - 1) // 2):
+        later.append(lax.ppermute(later[-1], axis, down))
+    line = jnp.concatenate([*earlier[::-1], *later[1:]], axis=dim)
+    return jnp.roll(line, (lax.axis_index(axis) - ways // 2) * x.shape[dim], axis=dim)
 
 
 def laid_out(pieces, dim):
@@ -52,7 +65,7 @@
 
 
 def gather_rows(normed):
-    return lax.all_gather(normed, "tp", axis=0, tiled=True)
+    return ring_gather(normed, "tp", 0)
 
 
 def add_piece(normed, shard_piece):

time: 463 us -> 468 us (1.011)
  blocking collectives: 114 us -> 55.6 us
  starting transfers between devices: 33 us -> 63.6 us
  waiting for transfers between devices: 218 us -> 230 us
  local copies, waits for them, and re-layouts: 4.77 us -> 14.1 us
  other arithmetic: 15.7 us -> 23.4 us
    all_to_all x2 -> x1, blocking collectives: 114 us -> 55.6 us  [summed_on_arrival(): pieces = lax.all_to_all(split_up(array, dim, count), axis, 0, 0, tiled=True)]
    all_gather x2 -> x0, waiting for transfers between devices: 50.3 us -> none  [gather_rows(): return lax.all_gather(normed, 'tp', axis=0, tiled=True)]
    all_to_all x0 -> x1, waiting for transfers between devices: none -> 48 us  [summed_on_arrival(): pieces = lax.all_to_all(split_up(array, dim, count), axis, 0, 0, tiled=True)]
    ppermute x0 -> x14, waiting for transfers between devices: none -> 44.8 us  [the longest x8 39.7 us: ring_gather(): earlier.append(lax.ppermute(earlier[-1], axis, up))]
    ppermute x0 -> x14, starting transfers between devices: none -> 36.7 us  [the longest x6 25.1 us: ring_gather(): later.append(lax.ppermute(later[-1], axis, down))]
    all_gather x2, waiting for transfers between devices: 131 us -> 113 us  [sent_together(): lax.all_gather(both, axis, axis=dim, tiled=True)]
    all_to_all x2, starting transfers between devices: 32.7 us -> 18.3 us  [from_everyone(): return lax.all_to_all(copies, axis, split_axis=0, concat_axis=0, tiled=True)]
    all_to_all x2, waiting for transfers between devices: 37.1 us -> 24.1 us  [from_everyone(): return lax.all_to_all(copies, axis, split_axis=0, concat_axis=0, tiled=True)]
  transfers between devices with their start and end apart: 6 -> 19, of which waited for: 4 -> 14; matrix products, arithmetic and copies ran while one was open for 14% -> 18% of each run, Pallas kernels for 0% -> 0%
where the time goes in v1:
time: 468 us; the launch traced here: 467 us
  waiting for transfers between devices  230 us (49%)
  matrix products  66.3 us (14%)
  starting transfers between devices  63.6 us (14%)
  blocking collectives  55.6 us (12%)
  other arithmetic  23.4 us (5%)
  local copies, waits for them, and re-layouts  14.1 us (3%)
  between operations  13.8 us (3%)
    all_gather x2, waiting for transfers between devices, sent_together(): lax.all_gather(both, axis, axis=dim, tiled=True)  113 us
    all_to_all x1, blocking collectives, summed_on_arrival(): pieces = lax.all_to_all(split_up(array, dim, count), axis, 0, 0, tiled=True)  55.6 us
    all_to_all x1, waiting for transfers between devices, summed_on_arrival(): pieces = lax.all_to_all(split_up(array, dim, count), axis, 0, 0, tiled=True)  48 us
    ppermute x8, waiting for transfers between devices, ring_gather(): earlier.append(lax.ppermute(earlier[-1], axis, up))  39.7 us
    ppermute x6, starting transfers between devices, ring_gather(): later.append(lax.ppermute(later[-1], axis, down))  25.1 us
    all_to_all x2, waiting for transfers between devices, from_everyone(): return lax.all_to_all(copies, axis, split_axis=0, concat_axis=0, tiled=True)  24.1 us
    all_to_all x2, starting transfers between devices, from_everyone(): return lax.all_to_all(copies, axis, split_axis=0, concat_axis=0, tiled=True)  18.3 us
    dot_general x4, matrix products, add_piece(): return jnp.dot(normed, shard_piece, preferred_element_type=jnp.float32)  17.8 us
  transfers between devices with their start and end apart: 19, of which 14 were waited for; matrix products, arithmetic and copies ran while one was open for 18% of the time, Pallas kernels for 0%

profile of v1, /device:TPU:33, one launch (start us, length us, event | category | flops | bytes accessed | tf_op | source)
XLA Modules:
  0.0 467.1 jit_solution(384787997198761846)
XLA Ops:
  6.6 1.8 pad_maximum_fusion.1
  11.8 2.7 collective-permute-start
  14.5 19.2 %collective-permute-done = bf16[128,2048]{1,0:T(8,128)(2,1)S(1)} collective-permute-done((bf16[128,2048]{1,0:T(8,128)(2,1)S(1)}, bf16[128,2048]{1,0:T(8,128)(2,1)S(1)}, u32[]{:S(2)}, u32[]{:S(2)}) %collective-permute-start) | collective-permute-done | bytes 524320 | tf_op jit(solution)/shard_map/ppermute | solution.py:19
  33.7 8.4 %collective-permute-start.4 = (bf16[128,2048]{1,0:T(8,128)(2,1)S(1)}, bf16[128,2048]{1,0:T(8,128)(2,1)S(1)}, u32[]{:S(2)}, u32[]{:S(2)}) collective-permute-start(bf16[128,2048]{1,0:T(8,128)(2,1)S(1)} %fusion.41), channel_id=1, source_target_pairs={{0,7},{1,0},{2,1},{3,2},{4,3},{5,4},{6,5},{7,6},{8,15},{9,8},{10,9... | collective-permute-start | bytes 1572872 | tf_op jit(solution)/shard_map/ppermute | solution.py:21
  42.1 1.4 collective-permute-done.1
  43.6 8.3 %collective-permute-start.5 = (bf16[128,2048]{1,0:T(8,128)(2,1)S(1)}, bf16[128,2048]{1,0:T(8,128)(2,1)S(1)}, u32[]{:S(2)}, u32[]{:S(2)}) collective-permute-start(bf16[128,2048]{1,0:T(8,128)(2,1)S(1)} %collective-permute-done.4), channel_id=1, source_target_pairs={{0,7},{1,0},{2,1},{3,2},{4,3},{5,4},{6,5},{7,6},{8,15},{9,8},{10,9... | collective-permute-start | bytes 1572872 | tf_op jit(solution)/shard_map/ppermute | solution.py:21
  51.9 1.5 collective-permute-done.2
  54.5 1.5 broadcast_in_dim.19
  56.0 10.8 %all-to-all-start = ((bf16[16,512,128]{1,2,0:T(8,128)(2,1)}), bf16[16,512,128]{1,2,0:T(8,128)(2,1)}, u32[]{:S(2)}, u32[]{:S(2)}) async-start(bf16[16,512,128]{1,2,0:T(8,128)(2,1)} %broadcast_in_dim.19), calls=%async_computation | async-start | bytes 4194304 | tf_op jit(solution)/shard_map/all_to_all | solution.py:34
  67.1 2.7 collective-permute-start.6
  72.4 3.7 collective-permute-done.6
  76.2 5.7 %fusion.22 = bf16[1024,2048]{1,0:T(8,128)(2,1)} fusion(s32[]{:T(128)S(6)} %select_n.24, bf16[1024,2048]{1,0:T(8,128)(2,1)S(1)} %constant_dynamic-update-slice_fusion), kind=kLoop, calls=%fused_computation.31 | loop fusion | flops 8388608 | bytes 8388612 | tf_op jit(solution)/shard_map/jit(_roll_dynamic)/concatenate | solution.py:23
  82.0 112.8 %all-gather.3.cloned.1.call-done = bf16[2048,1536]{1,0:T(8,128)(2,1)} async-done(((bf16[128,1536]{1,0:T(8,128)(2,1)}), bf16[2048,1536]{1,0:T(8,128)(2,1)}) %all-gather.3.cloned.1.call-update) | async-done | bytes 6291472 | tf_op jit(solution)/shard_map/all_gather | solution.py:58
  194.8 3.9 convolution_bitcast_fusion.2
  198.7 2.5 convolution_bitcast_fusion.3
  201.2 2.3 subtract_convert_fusion
  205.6 4.9 %fusion.36 = bf16[1024,512]{1,0:T(8,128)(2,1)} fusion(bf16[1024,2048]{1,0:T(8,128)(2,1)S(1)} %copy-done.2, bf16[2048,1536]{1,0:T(8,128)(2,1)} %all-gather.3.cloned.1.call-done), kind=kOutput, calls=%fused_computation.52 | convolution fusion | flops 2148007936 | bytes 7340032 | tf_op jit(solution)/shard_map/dot_general | solution.py:72
  210.5 25.5 %while.15 = (s32[]{:T(128)}, f32[1,256,512]{2,1,0:T(8,128)S(1)}, f32[8,128,1,512]{3,1,2,0:T(8,128)}, f32[1]{0:T(128)}, bf16[8,128,1,256]{3,2,1,0:T(2,128)(2,1)S(...) while((s32[]{:T(128)}, f32[1,256,512]{2,1,0:T(8,128)S(1)}, ...), condition=%wide.region_2.4_spmd.clone.clone.clone, body=%wide.region_1.3_spmd.clone.clone.clone.sunk | while | flops 67797504 | bytes 2232440 | solution.py:132
  210.5 1.8 fusion.102
  213.7 1.8 fusion.102
  216.8 1.7 fusion.102
  220.0 1.7 fusion.102
  223.2 1.7 fusion.102
  226.3 1.7 fusion.102
  229.5 1.7 fusion.102
  232.7 1.7 fusion.102
  236.0 2.8 fusion.78
  239.2 6.5 %fusion.29 = bf16[1024,512]{1,0:T(8,128)(2,1)} fusion(f32[8,128,1,512]{3,1,0,2:T(8,128)S(1)} %get-tuple-element.180, bf16[1024,2048]{1,0:T(8,128)(2,1)} %fusion.22, bf16[2048,1536]{1,0:T(8,128)(2,1)} %all-gather.3.cloned.1.call-done, f32[1024]{0:T(1024)S(1)} %rsqrt_bitcast_fusion, f32[1024]{0:T(1024)S(1)} %get-tuple-element.175), kind=kOutput, calls=%fused_computation.42 | convolution fusion | flops 2151677952 | bytes 9445376 | tf_op jit(solution)/shard_map/dot_general | solution.py:72
  245.8 6.2 %convolution_convert_fusion.1 = bf16[1024,2048]{1,0:T(8,128)(2,1)} fusion(bf16[1024,512]{1,0:T(8,128)(2,1)} %fusion.29, bf16[512,2048]{0,1:T(8,128)(2,1)} %bitcast.26), kind=kOutput, calls=%fused_computation.33 | convolution fusion | flops 2149580800 | bytes 7340032 | tf_op jit(solution)/shard_map/dot_general | solution.py:78
  252.0 8.5 %all-to-all-start.1 = ((bf16[8,128,2048]{2,1,0:T(8,128)(2,1)}), bf16[8,128,2048]{2,1,0:T(8,128)(2,1)}, u32[]{:S(2)}, u32[]{:S(2)}) async-start(bf16[8,128,2048]{2,1,0:T(8,128)(2,1)} %bitcast.127), calls=%async_computation.1 | async-start | bytes 8388608 | tf_op jit(solution)/shard_map/all_to_all | solution.py:48
  261.5 48.0 %all-to-all-done.1 = bf16[8,128,2048]{2,1,0:T(8,128)(2,1)} async-done(((bf16[8,128,2048]{2,1,0:T(8,128)(2,1)}), bf16[8,128,2048]{2,1,0:T(8,128)(2,1)}, u32[]{:S(2)}, u32[]{:S(2)}) %all-to-all-start.1) | async-done | bytes 4194336 | tf_op jit(solution)/shard_map/all_to_all | solution.py:48
  309.4 1.4 broadcast_in_dim.20
  310.8 7.5 %all-to-all-start.2 = ((bf16[16,384,128]{1,2,0:T(8,128)(2,1)}), bf16[16,384,128]{1,2,0:T(8,128)(2,1)S(1)}, u32[]{:S(2)}, u32[]{:S(2)}) async-start(bf16[16,384,128]{1,2,0:T(8,128)(2,1)} %broadcast_in_dim.20), calls=%async_computation.2 | async-start | bytes 3145728 | tf_op jit(solution)/shard_map/all_to_all | solution.py:34
  318.3 3.0 convert_reduce_fusion.1
  322.2 1.5 collective-permute-start.7
  323.7 6.1 %collective-permute-done.7 = bf16[128,2048]{1,0:T(8,128)(2,1)S(1)} collective-permute-done((bf16[128,2048]{1,0:T(8,128)(2,1)S(1)}, bf16[128,2048]{1,0:T(8,128)(2,1)S(1)}, u32[]{:S(2)}, u32[]{:S(2)}) %collective-permute-start.7) | collective-permute-done | bytes 524320 | tf_op jit(solution)/shard_map/ppermute | solution.py:19
  329.8 2.5 collective-permute-start.8
  333.3 5.1 %collective-permute-done.8 = bf16[128,2048]{1,0:T(8,128)(2,1)S(1)} collective-permute-done((bf16[128,2048]{1,0:T(8,128)(2,1)S(1)}, bf16[128,2048]{1,0:T(8,128)(2,1)S(1)}, u32[]{:S(2)}, u32[]{:S(2)}) %collective-permute-start.8) | collective-permute-done | bytes 524320 | tf_op jit(solution)/shard_map/ppermute | solution.py:19
  338.4 2.5 collective-permute-start.9
  341.3 1.8 collective-permute-start.12
  343.1 3.9 collective-permute-done.9
  347.0 2.5 collective-permute-start.10
  350.3 2.9 collective-permute-start.13
  353.2 2.5 collective-permute-done.10
  362.4 6.3 %fusion.30 = f32[1024,384]{1,0:T(8,128)} fusion(bf16[2048,768]{1,0:T(8,128)(2,1)} %all-gather.5.cloned.1.call-done, s32[]{:T(128)S(6)} %select_n.24, bf16[1024,2048]{1,0:T(8,128)(2,1)} %constant_dynamic-update-slice_fusion.8), kind=kOutput, calls=%fused_computation.44 | convolution fusion | flops 1619001344 | bytes 7340036 | tf_op jit(solution)/shard_map/dot_general | solution.py:182
  368.7 24.1 %all-to-all-done.2 = bf16[16,384,128]{1,2,0:T(8,128)(2,1)S(1)} async-done(((bf16[16,384,128]{1,2,0:T(8,128)(2,1)}), bf16[16,384,128]{1,2,0:T(8,128)(2,1)S(1)}, u32[]{:S(2)}, u32[]{:S(2)}) %all-to-all-start.2) | async-done | bytes 1572896 | tf_op jit(solution)/shard_map/all_to_all | solution.py:34
  392.8 9.8 %convolution_convert_fusion = bf16[1024,2048]{1,0:T(8,128)(2,1)} fusion(bf16[384,2048]{0,1:T(8,128)(2,1)S(1)} %bitcast.135, f32[1024,384]{1,0:T(8,128)} %fusion.30, bf16[2048,768]{1,0:T(8,128)(2,1)} %all-gather.5.cloned.1.call-done, s32[]{:T(128)S(6)} %select_n.24, bf16[1024,2048]{1,0:T(8,128)(2,1)} %constant_dynamic-update-slice_fusion.8), kind=kOutput, calls=%fused_computation.32 | convolution fusion | flops 3234070528 | bytes 13107204 | tf_op jit(solution)/shard_map/dot_general | solution.py:78
  402.6 55.6 %all_to_all.20 = bf16[8,128,2048]{2,1,0:T(8,128)(2,1)S(1)} all-to-all(bf16[8,128,2048]{2,1,0:T(8,128)(2,1)} %bitcast.128), channel_id=1, replica_groups=mesh['grp'=2,'fs'=16,'tp'=8] {'tp'}, dimensions={0} | all-to-all | bytes 8388608 | tf_op jit(solution)/shard_map/all_to_all | solution.py:48
  (96 shorter events, 33.6 us)
Async XLA Ops:
  6.5 188.3 %all-gather.3.cloned.1.call-start = ((), (), s32[]{:S(2)}) async-start(), calls=%async_computation.4 | async-start | bytes 6684672 | tf_op jit(solution)/shard_map/all_gather | solution.py:58
  11.8 21.9 %collective-permute-start = (bf16[128,2048]{1,0:T(8,128)(2,1)S(1)}, bf16[128,2048]{1,0:T(8,128)(2,1)S(1)}, u32[]{:S(2)}, u32[]{:S(2)}) collective-permute-start(bf16[128,2048]{1,0:T(8,128)(2,1)S(1)} %fusion.41), channel_id=1, source_target_pairs={{0,1},{1,2},{2,3},{3,4},{4,5},{5,6},{6,7},{7,0},{8,9},{9,10},{10,1... | collective-permute-start | bytes 1572872 | tf_op jit(solution)/shard_map/ppermute | solution.py:19
  33.7 9.8 %collective-permute-start.1 = (bf16[128,2048]{1,0:T(8,128)(2,1)S(1)}, bf16[128,2048]{1,0:T(8,128)(2,1)S(1)}, u32[]{:S(2)}, u32[]{:S(2)}) collective-permute-start(bf16[128,2048]{1,0:T(8,128)(2,1)S(1)} %collective-permute-done), channel_id=1, source_target_pairs={{0,1},{1,2},{2,3},{3,4},{4,5},{5,6},{6,7},{7,0},{8,9},{9,10},{10,1... | collective-permute-start | bytes 1572872 | tf_op jit(solution)/shard_map/ppermute | solution.py:19
  33.7 9.9 %collective-permute-start.4 = (bf16[128,2048]{1,0:T(8,128)(2,1)S(1)}, bf16[128,2048]{1,0:T(8,128)(2,1)S(1)}, u32[]{:S(2)}, u32[]{:S(2)}) collective-permute-start(bf16[128,2048]{1,0:T(8,128)(2,1)S(1)} %fusion.41), channel_id=1, source_target_pairs={{0,7},{1,0},{2,1},{3,2},{4,3},{5,4},{6,5},{7,6},{8,15},{9,8},{10,9... | collective-permute-start | bytes 1572872 | tf_op jit(solution)/shard_map/ppermute | solution.py:21
  43.5 9.9 %collective-permute-start.2 = (bf16[128,2048]{1,0:T(8,128)(2,1)S(1)}, bf16[128,2048]{1,0:T(8,128)(2,1)}, u32[]{:S(2)}, u32[]{:S(2)}) collective-permute-start(bf16[128,2048]{1,0:T(8,128)(2,1)S(1)} %collective-permute-done.1), channel_id=1, source_target_pairs={{0,1},{1,2},{2,3},{3,4},{4,5},{5,6},{6,7},{7,0},{8,9},{9,10},{10,1... | collective-permute-start | bytes 1572872 | tf_op jit(solution)/shard_map/ppermute | solution.py:19
  43.6 23.5 %collective-permute-start.5 = (bf16[128,2048]{1,0:T(8,128)(2,1)S(1)}, bf16[128,2048]{1,0:T(8,128)(2,1)S(1)}, u32[]{:S(2)}, u32[]{:S(2)}) collective-permute-start(bf16[128,2048]{1,0:T(8,128)(2,1)S(1)} %collective-permute-done.4), channel_id=1, source_target_pairs={{0,7},{1,0},{2,1},{3,2},{4,3},{5,4},{6,5},{7,6},{8,15},{9,8},{10,9... | collective-permute-start | bytes 1572872 | tf_op jit(solution)/shard_map/ppermute | solution.py:21
  53.4 16.4 %collective-permute-start.3 = (bf16[128,2048]{1,0:T(8,128)(2,1)}, bf16[128,2048]{1,0:T(8,128)(2,1)}, u32[]{:S(2)}, u32[]{:S(2)}) collective-permute-start(bf16[128,2048]{1,0:T(8,128)(2,1)} %collective-permute-done.2), channel_id=1, source_target_pairs={{0,1},{1,2},{2,3},{3,4},{4,5},{5,6},{6,7},{7,0},{8,9},{9,10},{10,1... | collective-permute-start | bytes 1572872 | tf_op jit(solution)/shard_map/ppermute | solution.py:19
  56.0 16.1 %copy-start = (bf16[128,2048]{1,0:T(8,128)(2,1)S(1)}, bf16[128,2048]{1,0:T(8,128)(2,1)}, u32[]{:S(2)}) copy-start(bf16[128,2048]{1,0:T(8,128)(2,1)} %param.14) | copy-start | bytes 1572868
  56.0 189.8 %all-to-all-start = ((bf16[16,512,128]{1,2,0:T(8,128)(2,1)}), bf16[16,512,128]{1,2,0:T(8,128)(2,1)}, u32[]{:S(2)}, u32[]{:S(2)}) async-start(bf16[16,512,128]{1,2,0:T(8,128)(2,1)} %broadcast_in_dim.19), calls=%async_computation | async-start | bytes 4194304 | tf_op jit(solution)/shard_map/all_to_all | solution.py:34
  67.1 9.1 %collective-permute-start.6 = (bf16[128,2048]{1,0:T(8,128)(2,1)S(1)}, bf16[128,2048]{1,0:T(8,128)(2,1)S(1)}, u32[]{:S(2)}, u32[]{:S(2)}) collective-permute-start(bf16[128,2048]{1,0:T(8,128)(2,1)S(1)} %collective-permute-done.5), channel_id=1, source_target_pairs={{0,7},{1,0},{2,1},{3,2},{4,3},{5,4},{6,5},{7,6},{8,15},{9,8},{10,9... | collective-permute-start | bytes 1572872 | tf_op jit(solution)/shard_map/ppermute | solution.py:21
  194.8 3.9 copy-start.2
  203.5 1.0 copy-start.3
  203.5 7.0 %copy-start.1 = (f32[1024,1,128]{2,0,1:T(8,128)}, f32[1024,1,128]{2,0,1:T(8,128)S(1)}, u32[]{:S(2)}) copy-start(f32[1024,1,128]{2,0,1:T(8,128)S(1)} %get-tuple-element.178) | copy-start | bytes 1572868
  252.0 8.6 %copy-start.5 = (bf16[128,384]{1,0:T(8,128)(2,1)S(1)}, bf16[128,384]{1,0:T(8,128)(2,1)}, u32[]{:S(2)}) copy-start(bf16[128,384]{1,0:T(8,128)(2,1)} %param.22) | copy-start | bytes 294916
  252.0 8.6 %copy-start.6 = (bf16[128,384]{1,0:T(8,128)(2,1)S(1)}, bf16[128,384]{1,0:T(8,128)(2,1)}, u32[]{:S(2)}) copy-start(bf16[128,384]{1,0:T(8,128)(2,1)} %param.21) | copy-start | bytes 294916
  252.0 9.3 %copy-start.4 = (bf16[384,128]{1,0:T(8,128)(2,1)S(1)}, bf16[384,128]{1,0:T(8,128)(2,1)}, u32[]{:S(2)}) copy-start(bf16[384,128]{1,0:T(8,128)(2,1)} %param.23) | copy-start | bytes 294916
  252.0 57.4 %all-to-all-start.1 = ((bf16[8,128,2048]{2,1,0:T(8,128)(2,1)}), bf16[8,128,2048]{2,1,0:T(8,128)(2,1)}, u32[]{:S(2)}, u32[]{:S(2)}) async-start(bf16[8,128,2048]{2,1,0:T(8,128)(2,1)} %bitcast.127), calls=%async_computation.1 | async-start | bytes 8388608 | tf_op jit(solution)/shard_map/all_to_all | solution.py:48
  260.6 101.9 %all-gather.5.cloned.1.call-start = ((), (), s32[]{:S(2)}) async-start(), calls=%async_computation.5 | async-start | bytes 3342336 | tf_op jit(solution)/shard_map/all_gather | solution.py:58
  310.8 82.0 %all-to-all-start.2 = ((bf16[16,384,128]{1,2,0:T(8,128)(2,1)}), bf16[16,384,128]{1,2,0:T(8,128)(2,1)S(1)}, u32[]{:S(2)}, u32[]{:S(2)}) async-start(bf16[16,384,128]{1,2,0:T(8,128)(2,1)} %broadcast_in_dim.20), calls=%async_computation.2 | async-start | bytes 3145728 | tf_op jit(solution)/shard_map/all_to_all | solution.py:34
  322.2 7.6 %collective-permute-start.7 = (bf16[128,2048]{1,0:T(8,128)(2,1)S(1)}, bf16[128,2048]{1,0:T(8,128)(2,1)S(1)}, u32[]{:S(2)}, u32[]{:S(2)}) collective-permute-start(bf16[128,2048]{1,0:T(8,128)(2,1)S(1)} %multiply_convert_fusion.1), channel_id=1, source_target_pairs={{0,1},{1,2},{2,3},{3,4},{4,5},{5,6},{6,7},{7,0},{8,9},{9,10},{10,1... | collective-permute-start | bytes 1572872 | tf_op jit(solution)/shard_map/ppermute | solution.py:19
  329.8 8.6 %collective-permute-start.8 = (bf16[128,2048]{1,0:T(8,128)(2,1)S(1)}, bf16[128,2048]{1,0:T(8,128)(2,1)S(1)}, u32[]{:S(2)}, u32[]{:S(2)}) collective-permute-start(bf16[128,2048]{1,0:T(8,128)(2,1)S(1)} %collective-permute-done.7), channel_id=1, source_target_pairs={{0,1},{1,2},{2,3},{3,4},{4,5},{5,6},{6,7},{7,0},{8,9},{9,10},{10,1... | collective-permute-start | bytes 1572872 | tf_op jit(solution)/shard_map/ppermute | solution.py:19
  332.3 9.0 %collective-permute-start.11 = (bf16[128,2048]{1,0:T(8,128)(2,1)S(1)}, bf16[128,2048]{1,0:T(8,128)(2,1)S(1)}, u32[]{:S(2)}, u32[]{:S(2)}) collective-permute-start(bf16[128,2048]{1,0:T(8,128)(2,1)S(1)} %multiply_convert_fusion.1), channel_id=1, source_target_pairs={{0,7},{1,0},{2,1},{3,2},{4,3},{5,4},{6,5},{7,6},{8,15},{9,8},{10,9... | collective-permute-start | bytes 1572872 | tf_op jit(solution)/shard_map/ppermute | solution.py:21
  338.4 8.6 %collective-permute-start.9 = (bf16[128,2048]{1,0:T(8,128)(2,1)S(1)}, bf16[128,2048]{1,0:T(8,128)(2,1)S(1)}, u32[]{:S(2)}, u32[]{:S(2)}) collective-permute-start(bf16[128,2048]{1,0:T(8,128)(2,1)S(1)} %collective-permute-done.8), channel_id=1, source_target_pairs={{0,1},{1,2},{2,3},{3,4},{4,5},{5,6},{6,7},{7,0},{8,9},{9,10},{10,1... | collective-permute-start | bytes 1572872 | tf_op jit(solution)/shard_map/ppermute | solution.py:19
  341.3 9.0 %collective-permute-start.12 = (bf16[128,2048]{1,0:T(8,128)(2,1)S(1)}, bf16[128,2048]{1,0:T(8,128)(2,1)S(1)}, u32[]{:S(2)}, u32[]{:S(2)}) collective-permute-start(bf16[128,2048]{1,0:T(8,128)(2,1)S(1)} %collective-permute-done.11), channel_id=1, source_target_pairs={{0,7},{1,0},{2,1},{3,2},{4,3},{5,4},{6,5},{7,6},{8,15},{9,8},{10,9... | collective-permute-start | bytes 1572872 | tf_op jit(solution)/shard_map/ppermute | solution.py:21
  347.0 8.6 %collective-permute-start.10 = (bf16[128,2048]{1,0:T(8,128)(2,1)S(1)}, bf16[128,2048]{1,0:T(8,128)(2,1)S(1)}, u32[]{:S(2)}, u32[]{:S(2)}) collective-permute-start(bf16[128,2048]{1,0:T(8,128)(2,1)S(1)} %collective-permute-done.9), channel_id=1, source_target_pairs={{0,1},{1,2},{2,3},{3,4},{4,5},{5,6},{6,7},{7,0},{8,9},{9,10},{10,1... | collective-permute-start | bytes 1572872 | tf_op jit(solution)/shard_map/ppermute | solution.py:19
  350.3 11.2 %collective-permute-start.13 = (bf16[128,2048]{1,0:T(8,128)(2,1)S(1)}, bf16[128,2048]{1,0:T(8,128)(2,1)S(1)}, u32[]{:S(2)}, u32[]{:S(2)}) collective-permute-start(bf16[128,2048]{1,0:T(8,128)(2,1)S(1)} %collective-permute-done.12), channel_id=1, source_target_pairs={{0,7},{1,0},{2,1},{3,2},{4,3},{5,4},{6,5},{7,6},{8,15},{9,8},{10,9... | collective-permute-start | bytes 1572872 | tf_op jit(solution)/shard_map/ppermute | solution.py:21
Sparse Core Ops, SparseCore 0:
  9.1 185.6 all-gather.2
  263.2 73.0 all-gather.4
